TPU v7x, 512 devices: a whole 4x4x16 slice. The times are simulated.
512 devices in a mesh: gr: 2 (over z_hi), fs: 32 (over z_lo, y), tp: 8 (over x, core).
Axes of the slice: x: 4, y: 4, z: 16 (z_hi: 2, z_lo: 8; z = z_hi * 8 + z_lo), core: 2. Of those that a mesh axis runs over, the one named last changes fastest.
Arguments:
- prompt: bfloat16 [8192, 2048], P(('gr', 'tp'), 'fs'), may hold values from -2.5 to 2.5
- gain_pre: float32 [2048], P(('gr', 'fs')), may hold values from 0.1 to 1.9
- gate_pre: float32 [2048, 5632], P(('gr', 'fs'), 'tp'), may hold values from -6 to 6
- up_pre: float32 [2048, 5632], P(('gr', 'fs'), 'tp'), may hold values from -6 to 6
- down_pre: float32 [2048, 5632], P(('gr', 'fs'), 'tp'), may hold values from -16 to 16
- gain_post: float32 [2048], P(('gr', 'fs')), may hold values from 0.1 to 1.9
- gate_post: float32 [2048, 5632], P(('gr', 'fs'), 'tp'), may hold values from -6 to 6
- up_post: float32 [2048, 5632], P(('gr', 'fs'), 'tp'), may hold values from -6 to 6
- down_post: float32 [2048, 5632], P(('gr', 'fs'), 'tp'), may hold values from -16 to 16
Outputs:
- result: bfloat16 [8192, 2048], P(('gr', 'tp'), 'fs')
- gate_first: bfloat16 [5632, 2048], P('fs')
- up_first: bfloat16 [5632, 2048], P('fs')
- down_first: bfloat16 [5632, 2048], P('fs')
- gate_second: bfloat16 [5632, 2048], P('fs')
- up_second: bfloat16 [5632, 2048], P('fs')
- down_second: bfloat16 [5632, 2048], P('fs')
All inputs are finite; a program needn't handle non-finite values.
Results may differ from a plain program's by a relative error of at most 0.028.
Values may be sent and summed in bfloat16 or wider, within the bound.
No kernel may reach another device: no remote copies, remote signals or barrier semaphores. Data moves between devices by JAX's collectives and lax.ppermute only.
A program may use at most 64 MiB of HBM per device.

v0:
```python
import jax
import jax.numpy as jnp
from jax import lax
from jax.sharding import PartitionSpec as P

D = 2048
FF = 5632


norm_eps = 1e-06


def copy_for_each(shard, axis):
    copies = jnp.broadcast_to(shard, (lax.axis_size(axis), *shard.shape))
    return lax.all_to_all(copies, axis, split_axis=0, concat_axis=0, tiled=True)


def laid_out(blocks, dim):
    dims = list(blocks.shape[1:])
    dims[dim] *= blocks.shape[0]
    return jnp.moveaxis(blocks, 0, dim).reshape(dims)


def gathered_copies(shard, axis, dim):
    blocks = copy_for_each(shard, axis)
    return laid_out(blocks, dim)


def in_blocks(shard, dim, size):
    dims = shard.shape
    blocks = shard.reshape(*dims[:dim], size, dims[dim] // size, *dims[dim + 1 :])
    return jnp.moveaxis(blocks, dim, 0)


def summed_on_arrival(shard, axis, dim):
    size = lax.axis_size(axis)
    blocks = lax.all_to_all(in_blocks(shard, dim, size), axis, 0, 0, tiled=True)
    return jnp.sum(blocks.astype(jnp.float32), axis=0)


def in_one_piece(arrays, axis, dim, along):
    ends, at = ([], 0)
    for a in arrays[:-1]:
        at += a.shape[along]
        ends.append(at)
    both = jnp.concatenate(arrays, axis=along)
    return tuple(jnp.split(lax.all_gather(both, axis, axis=dim, tiled=True), ends, axis=along))


def add_products(columns_in, w_gate, w_up):
    widened = columns_in.astype(jnp.float32)
    dims = (((1,), (1,)), ((), ()))
    return (
        lax.dot_general(columns_in, w_gate, dims, preferred_element_type=jnp.float32),
        lax.dot_general(columns_in, w_up, dims, preferred_element_type=jnp.float32),
        jnp.sum(widened * widened, axis=1),
    )


def half_step(tokens, w_gate, w_up, w_down):
    gate_sum, up_sum, squares = add_products(gathered_copies(tokens, "fs", 1), w_gate, w_up)
    row_scale = (lax.rsqrt(squares / D + norm_eps) * D ** (-0.5))[:, None]
    hidden = (jax.nn.silu(gate_sum * row_scale) * (up_sum * row_scale)).astype(jnp.bfloat16)
    partial_value = jnp.dot(hidden, w_down, preferred_element_type=jnp.float32)
    summed = summed_on_arrival(partial_value.astype(jnp.bfloat16), "fs", 1)
    return (tokens.astype(jnp.float32) + 0.5 * FF ** (-0.5) * summed).astype(jnp.bfloat16)


def restore_rows(matrix, groups, shards, lanes):
    row_total, col_total = matrix.shape
    sub_rows = row_total // (groups * shards * lanes)
    shaped = matrix.reshape(groups, lanes, shards, sub_rows, col_total)
    return jnp.transpose(shaped, (0, 2, 1, 3, 4)).reshape(row_total, col_total)


def relayout(matrices):
    crossed = (
        lax.all_to_all(
            lax.all_to_all(matrices[0], "tp", split_axis=0, concat_axis=1, tiled=True),
            "fs",
            split_axis=1,
            concat_axis=0,
            tiled=True,
        ),
        lax.all_to_all(
            lax.all_to_all(matrices[1], "tp", split_axis=0, concat_axis=1, tiled=True),
            "fs",
            split_axis=1,
            concat_axis=0,
            tiled=True,
        ),
        lax.all_to_all(
            lax.all_to_all(matrices[2], "tp", split_axis=0, concat_axis=1, tiled=True),
            "fs",
            split_axis=1,
            concat_axis=0,
            tiled=True,
        ),
        lax.all_to_all(
            lax.all_to_all(matrices[3], "tp", split_axis=0, concat_axis=1, tiled=True),
            "fs",
            split_axis=1,
            concat_axis=0,
            tiled=True,
        ),
        lax.all_to_all(
            lax.all_to_all(matrices[4], "tp", split_axis=0, concat_axis=1, tiled=True),
            "fs",
            split_axis=1,
            concat_axis=0,
            tiled=True,
        ),
        lax.all_to_all(
            lax.all_to_all(matrices[5], "tp", split_axis=0, concat_axis=1, tiled=True),
            "fs",
            split_axis=1,
            concat_axis=0,
            tiled=True,
        ),
    )
    gathered = in_one_piece(
        (crossed[0], crossed[1], crossed[2], crossed[3], crossed[4], crossed[5]), ("gr", "tp"), 0, 1
    )
    groups = lax.axis_size("gr")
    shards = lax.axis_size("fs")
    lanes = lax.axis_size("tp")
    return tuple((restore_rows(matrix, groups, shards, lanes).T for matrix in gathered))


def local(prompt, gain_pre, gate_pre, up_pre, down_pre, gain_post, gate_post, up_post, down_post):
    rounded = (
        (gain_pre[:, None] * gate_pre).astype(jnp.bfloat16),
        (gain_pre[:, None] * up_pre).astype(jnp.bfloat16),
        down_pre.astype(jnp.bfloat16),
        (gain_post[:, None] * gate_post).astype(jnp.bfloat16),
        (gain_post[:, None] * up_post).astype(jnp.bfloat16),
        down_post.astype(jnp.bfloat16),
    )
    served = relayout(rounded)
    middle = half_step(prompt, served[0], served[1], served[2])
    result = half_step(middle, served[3], served[4], served[5])
    return (result, served[0], served[1], served[2], served[3], served[4], served[5])


def solution(mesh):
    placed = (
        P(("gr", "tp"), "fs"),
        P(("gr", "fs")),
        P(("gr", "fs"), "tp"),
        P(("gr", "fs"), "tp"),
        P(("gr", "fs"), "tp"),
        P(("gr", "fs")),
        P(("gr", "fs"), "tp"),
        P(("gr", "fs"), "tp"),
        P(("gr", "fs"), "tp"),
    )
    return jax.shard_map(
        local,
        mesh=mesh,
        in_specs=placed,
        out_specs=(
            P(("gr", "tp"), "fs"),
            P("fs", None),
            P("fs", None),
            P("fs", None),
            P("fs", None),
            P("fs", None),
            P("fs", None),
        ),
        check_vma=False,
    )
```

profile of v0, /device:TPU:6, one launch (start us, length us, event | category | flops | bytes accessed | tf_op | source)
XLA Modules:
  0.0 711.1 jit_solution(13463120241691673238)
XLA Ops:
  8.8 9.1 %all-to-all-start = ((bf16[8,4,704]{2,1,0:T(4,128)(2,1)}), bf16[8,4,704]{2,1,0:T(4,128)(2,1)S(1)}, u32[]{:S(2)}, u32[]{:S(2)}) async-start(bf16[8,4,704]{2,1,0:T(4,128)(2,1)} %all_to_all.168), calls=%async_computation | async-start | bytes 98304 | tf_op jit(solution)/shard_map/all_to_all | solution.py:79
  18.6 2.8 all-to-all-done
  21.4 5.4 all-to-all-start.2
  30.2 5.4 all-to-all-start.6
  36.2 2.8 all-to-all-done.6
  39.0 5.4 all-to-all-start.8
  47.8 5.4 all-to-all-start.4
  56.6 5.4 all-to-all-start.10
  62.8 2.6 all-to-all-done.10
  65.4 11.2 %all-to-all-start.1 = ((bf16[4,32,176]{2,0,1:T(4,128)(2,1)}), bf16[4,32,176]{2,0,1:T(4,128)(2,1)S(1)}, u32[]{:S(2)}, u32[]{:S(2)}) async-start(bf16[4,32,176]{2,0,1:T(4,128)(2,1)} %copy.45), calls=%async_computation.1 | async-start | bytes 131072 | tf_op jit(solution)/shard_map/all_to_all | solution.py:78
  77.5 12.0 %all-to-all-done.1 = bf16[4,32,176]{2,0,1:T(4,128)(2,1)S(1)} async-done(((bf16[4,32,176]{2,0,1:T(4,128)(2,1)}), bf16[4,32,176]{2,0,1:T(4,128)(2,1)S(1)}, u32[]{:S(2)}, u32[]{:S(2)}) %all-to-all-start.1) | async-done | bytes 45088 | tf_op jit(solution)/shard_map/all_to_all | solution.py:78
  89.5 3.9 all-to-all-start.3
  94.2 12.0 %all-to-all-done.3 = bf16[4,32,176]{2,0,1:T(4,128)(2,1)S(1)} async-done(((bf16[4,32,176]{2,0,1:T(4,128)(2,1)}), bf16[4,32,176]{2,0,1:T(4,128)(2,1)S(1)}, u32[]{:S(2)}, u32[]{:S(2)}) %all-to-all-start.3) | async-done | bytes 45088 | tf_op jit(solution)/shard_map/all_to_all | solution.py:85
  106.3 3.9 all-to-all-start.7
  111.0 12.0 %all-to-all-done.7 = bf16[4,32,176]{2,0,1:T(4,128)(2,1)S(1)} async-done(((bf16[4,32,176]{2,0,1:T(4,128)(2,1)}), bf16[4,32,176]{2,0,1:T(4,128)(2,1)S(1)}, u32[]{:S(2)}, u32[]{:S(2)}) %all-to-all-start.7) | async-done | bytes 45088 | tf_op jit(solution)/shard_map/all_to_all | solution.py:99
  123.0 3.9 all-to-all-start.9
  127.7 12.0 %all-to-all-done.9 = bf16[4,32,176]{2,0,1:T(4,128)(2,1)S(1)} async-done(((bf16[4,32,176]{2,0,1:T(4,128)(2,1)}), bf16[4,32,176]{2,0,1:T(4,128)(2,1)S(1)}, u32[]{:S(2)}, u32[]{:S(2)}) %all-to-all-start.9) | async-done | bytes 45088 | tf_op jit(solution)/shard_map/all_to_all | solution.py:106
  139.7 3.9 all-to-all-start.5
  143.8 12.7 %all-to-all-done.5 = bf16[4,32,176]{2,0,1:T(4,128)(2,1)S(1)} async-done(((bf16[4,32,176]{2,0,1:T(4,128)(2,1)}), bf16[4,32,176]{2,0,1:T(4,128)(2,1)S(1)}, u32[]{:S(2)}, u32[]{:S(2)}) %all-to-all-start.5) | async-done | bytes 45088 | tf_op jit(solution)/shard_map/all_to_all | solution.py:92
  156.5 16.3 %all_to_all.230 = bf16[4,32,176]{2,0,1:T(4,128)(2,1)S(1)} all-to-all(bf16[4,32,176]{2,0,1:T(4,128)(2,1)S(1)} %copy.55), channel_id=1, replica_groups=mesh['gr'=2,'fs'=32,'tp'=8] {'fs'}, dimensions={1} | all-to-all | bytes 90112 | tf_op jit(solution)/shard_map/all_to_all | solution.py:113
  174.3 4.0 all-to-all-start.12
  179.8 143.7 %all-to-all-done.12 = bf16[32,512,64]{1,2,0:T(8,128)(2,1)S(1)} async-done(((bf16[32,512,64]{1,2,0:T(8,128)(2,1)}), bf16[32,512,64]{1,2,0:T(8,128)(2,1)S(1)}, u32[]{:S(2)}, u32[]{:S(2)}) %all-to-all-start.12) | async-done | bytes 2097184 | tf_op jit(solution)/shard_map/all_to_all | solution.py:15
  324.1 3.1 all-gather.2.cloned.1.call-done
  327.2 8.8 %fusion.22 = (bf16[2048,176]{1,0:T(8,128)(2,1)}, bf16[2048,176]{1,0:T(8,128)(2,1)S(1)}, bf16[2048,176]{1,0:T(8,128)(2,1)}, bf16[2048,176]{1,0:T(8,128)(2,1)}, bf...) fusion(bf16[2048,1056]{1,0:T(8,128)(2,1)} %all-gather.2.cloned.1.call-done), kind=kLoop, calls=%fused_computation.40 | loop fusion | bytes 8650752 | tf_op jit(solution)/shard_map/split | solution.py:47
  338.2 2.7 copy.56
  340.9 2.5 reshape.119
  345.6 2.7 copy.57
  348.4 2.5 reshape.122
  353.1 2.7 copy.58
  355.8 2.5 reshape.124
  358.4 2.5 fusion.3
  360.9 4.3 convolution_convert_fusion.1
  365.2 2.9 copy.59
  368.1 118.8 %all_to_all.231 = bf16[32,512,64]{1,2,0:T(8,128)(2,1)S(1)} all-to-all(bf16[32,512,64]{1,2,0:T(8,128)(2,1)S(1)} %bitcast.63), channel_id=1, replica_groups=mesh['gr'=2,'fs'=32,'tp'=8] {'fs'}, dimensions={0} | all-to-all | bytes 4194304 | tf_op jit(solution)/shard_map/all_to_all | solution.py:37
  488.7 6.6 all-to-all-start.14
  497.5 2.8 copy.60
  500.3 2.5 reshape.128
  504.9 2.8 copy.61
  507.7 2.5 reshape.130
  511.3 2.8 copy.62
  514.1 2.6 reshape.132
  516.7 73.8 %all-to-all-done.14 = bf16[32,512,64]{1,2,0:T(8,128)(2,1)S(1)} async-done(((bf16[32,512,64]{1,2,0:T(8,128)(2,1)}), bf16[32,512,64]{1,2,0:T(8,128)(2,1)S(1)}, u32[]{:S(2)}, u32[]{:S(2)}) %all-to-all-start.14) | async-done | bytes 2097184 | tf_op jit(solution)/shard_map/all_to_all | solution.py:15
  592.4 4.3 convolution_convert_fusion
  596.8 3.9 copy.63
  600.7 7.5 %all-to-all-start.15 = ((bf16[32,512,64]{1,2,0:T(8,128)(2,1)}), bf16[32,512,64]{1,2,0:T(8,128)(2,1)S(1)}, u32[]{:S(2)}, u32[]{:S(2)}) async-start(bf16[32,512,64]{1,2,0:T(8,128)(2,1)} %bitcast.62), calls=%async_computation.15 | async-start | bytes 4194304 | tf_op jit(solution)/shard_map/all_to_all | solution.py:37
  609.4 2.3 copy.65
  612.9 2.3 copy.67
  618.5 84.8 %all-to-all-done.15 = bf16[32,512,64]{1,2,0:T(8,128)(2,1)S(1)} async-done(((bf16[32,512,64]{1,2,0:T(8,128)(2,1)}), bf16[32,512,64]{1,2,0:T(8,128)(2,1)S(1)}, u32[]{:S(2)}, u32[]{:S(2)}) %all-to-all-start.15) | async-done | bytes 2097184 | tf_op jit(solution)/shard_map/all_to_all | solution.py:37
  (71 shorter events, 43.8 us)
Async XLA Ops:
  8.8 12.5 %all-to-all-start = ((bf16[8,4,704]{2,1,0:T(4,128)(2,1)}), bf16[8,4,704]{2,1,0:T(4,128)(2,1)S(1)}, u32[]{:S(2)}, u32[]{:S(2)}) async-start(bf16[8,4,704]{2,1,0:T(4,128)(2,1)} %all_to_all.168), calls=%async_computation | async-start | bytes 98304 | tf_op jit(solution)/shard_map/all_to_all | solution.py:79
  21.4 8.8 %all-to-all-start.2 = ((bf16[8,4,704]{2,1,0:T(4,128)(2,1)}), bf16[8,4,704]{2,1,0:T(4,128)(2,1)S(1)}, u32[]{:S(2)}, u32[]{:S(2)}) async-start(bf16[8,4,704]{2,1,0:T(4,128)(2,1)} %all_to_all.175), calls=%async_computation.2 | async-start | bytes 98304 | tf_op jit(solution)/shard_map/all_to_all | solution.py:86
  26.8 146.0 %copy-start.4 = (bf16[512,64]{0,1:T(8,128)(2,1)S(1)}, bf16[512,64]{0,1:T(8,128)(2,1)}, u32[]{:S(2)}) copy-start(bf16[512,64]{0,1:T(8,128)(2,1)} %param.9) | copy-start | bytes 196612
  30.2 8.8 %all-to-all-start.6 = ((bf16[8,4,704]{2,1,0:T(4,128)(2,1)}), bf16[8,4,704]{2,1,0:T(4,128)(2,1)S(1)}, u32[]{:S(2)}, u32[]{:S(2)}) async-start(bf16[8,4,704]{2,1,0:T(4,128)(2,1)} %all_to_all.189), calls=%async_computation.6 | async-start | bytes 98304 | tf_op jit(solution)/shard_map/all_to_all | solution.py:100
  39.0 8.8 %all-to-all-start.8 = ((bf16[8,4,704]{2,1,0:T(4,128)(2,1)}), bf16[8,4,704]{2,1,0:T(4,128)(2,1)S(1)}, u32[]{:S(2)}, u32[]{:S(2)}) async-start(bf16[8,4,704]{2,1,0:T(4,128)(2,1)} %all_to_all.196), calls=%async_computation.8 | async-start | bytes 98304 | tf_op jit(solution)/shard_map/all_to_all | solution.py:107
  47.8 8.8 %all-to-all-start.4 = ((bf16[8,4,704]{2,1,0:T(4,128)(2,1)}), bf16[8,4,704]{2,1,0:T(4,128)(2,1)S(1)}, u32[]{:S(2)}, u32[]{:S(2)}) async-start(bf16[8,4,704]{2,1,0:T(4,128)(2,1)} %all_to_all.182), calls=%async_computation.4 | async-start | bytes 98304 | tf_op jit(solution)/shard_map/all_to_all | solution.py:93
  56.6 8.8 %all-to-all-start.10 = ((bf16[8,4,704]{2,1,0:T(4,128)(2,1)}), bf16[8,4,704]{2,1,0:T(4,128)(2,1)S(1)}, u32[]{:S(2)}, u32[]{:S(2)}) async-start(bf16[8,4,704]{2,1,0:T(4,128)(2,1)} %all_to_all.203), calls=%async_computation.10 | async-start | bytes 98304 | tf_op jit(solution)/shard_map/all_to_all | solution.py:114
  65.4 24.1 %all-to-all-start.1 = ((bf16[4,32,176]{2,0,1:T(4,128)(2,1)}), bf16[4,32,176]{2,0,1:T(4,128)(2,1)S(1)}, u32[]{:S(2)}, u32[]{:S(2)}) async-start(bf16[4,32,176]{2,0,1:T(4,128)(2,1)} %copy.45), calls=%async_computation.1 | async-start | bytes 131072 | tf_op jit(solution)/shard_map/all_to_all | solution.py:78
  89.5 16.7 %all-to-all-start.3 = ((bf16[4,32,176]{2,0,1:T(4,128)(2,1)}), bf16[4,32,176]{2,0,1:T(4,128)(2,1)S(1)}, u32[]{:S(2)}, u32[]{:S(2)}) async-start(bf16[4,32,176]{2,0,1:T(4,128)(2,1)} %copy.47), calls=%async_computation.3 | async-start | bytes 131072 | tf_op jit(solution)/shard_map/all_to_all | solution.py:85
  106.3 16.7 %all-to-all-start.7 = ((bf16[4,32,176]{2,0,1:T(4,128)(2,1)}), bf16[4,32,176]{2,0,1:T(4,128)(2,1)S(1)}, u32[]{:S(2)}, u32[]{:S(2)}) async-start(bf16[4,32,176]{2,0,1:T(4,128)(2,1)} %copy.51), calls=%async_computation.7 | async-start | bytes 131072 | tf_op jit(solution)/shard_map/all_to_all | solution.py:99
  123.0 16.7 %all-to-all-start.9 = ((bf16[4,32,176]{2,0,1:T(4,128)(2,1)}), bf16[4,32,176]{2,0,1:T(4,128)(2,1)S(1)}, u32[]{:S(2)}, u32[]{:S(2)}) async-start(bf16[4,32,176]{2,0,1:T(4,128)(2,1)} %copy.53), calls=%async_computation.9 | async-start | bytes 131072 | tf_op jit(solution)/shard_map/all_to_all | solution.py:106
  139.7 16.7 %all-to-all-start.5 = ((bf16[4,32,176]{2,0,1:T(4,128)(2,1)}), bf16[4,32,176]{2,0,1:T(4,128)(2,1)S(1)}, u32[]{:S(2)}, u32[]{:S(2)}) async-start(bf16[4,32,176]{2,0,1:T(4,128)(2,1)} %copy.49), calls=%async_computation.5 | async-start | bytes 131072 | tf_op jit(solution)/shard_map/all_to_all | solution.py:92
  174.3 149.2 %all-to-all-start.12 = ((bf16[32,512,64]{1,2,0:T(8,128)(2,1)}), bf16[32,512,64]{1,2,0:T(8,128)(2,1)S(1)}, u32[]{:S(2)}, u32[]{:S(2)}) async-start(bf16[32,512,64]{1,2,0:T(8,128)(2,1)} %broadcast_in_dim.4), calls=%async_computation.12 | async-start | bytes 4194304 | tf_op jit(solution)/shard_map/all_to_all | solution.py:15
  178.4 148.8 %all-gather.2.cloned.1.call-start = ((), (), s32[]{:S(2)}) async-start(), calls=%async_computation.16 | async-start | bytes 5013504 | tf_op jit(solution)/shard_map/all_gather | solution.py:47
  488.7 101.8 %all-to-all-start.14 = ((bf16[32,512,64]{1,2,0:T(8,128)(2,1)}), bf16[32,512,64]{1,2,0:T(8,128)(2,1)S(1)}, u32[]{:S(2)}, u32[]{:S(2)}) async-start(bf16[32,512,64]{1,2,0:T(8,128)(2,1)} %broadcast_in_dim.5), calls=%async_computation.14 | async-start | bytes 4194304 | tf_op jit(solution)/shard_map/all_to_all | solution.py:15
  514.1 77.0 %copy-start.2 = (bf16[2048,176]{1,0:T(8,128)(2,1)S(1)}, bf16[2048,176]{1,0:T(8,128)(2,1)}, u32[]{:S(2)}) copy-start(bf16[2048,176]{1,0:T(8,128)(2,1)} %reshape.128) | copy-start | bytes 2162692
  600.7 7.5 %copy-start = (bf16[2048,176]{1,0:T(8,128)(2,1)S(1)}, bf16[2048,176]{1,0:T(8,128)(2,1)}, u32[]{:S(2)}) copy-start(bf16[2048,176]{1,0:T(8,128)(2,1)} %reshape.119) | copy-start | bytes 2162692
  600.7 102.6 %all-to-all-start.15 = ((bf16[32,512,64]{1,2,0:T(8,128)(2,1)}), bf16[32,512,64]{1,2,0:T(8,128)(2,1)S(1)}, u32[]{:S(2)}, u32[]{:S(2)}) async-start(bf16[32,512,64]{1,2,0:T(8,128)(2,1)} %bitcast.62), calls=%async_computation.15 | async-start | bytes 4194304 | tf_op jit(solution)/shard_map/all_to_all | solution.py:37
  609.4 2.3 copy-start.1
  612.9 2.3 copy-start.3
Sparse Core Ops, SparseCore 0:
  183.0 144.0 all-gather.1
where the time goes:
time: 713 us; the launch traced here: 711 us
  waiting for transfers between devices  380 us (53%)
  blocking collectives  135 us (19%)
  local copies, waits for them, and re-layouts  82.1 us (12%)
  starting transfers between devices  80.9 us (11%)
  between operations  14.3 us (2%)
  matrix products  12.5 us (2%)
    all_to_all x2, waiting for transfers between devices, copy_for_each(): return lax.all_to_all(copies, axis, split_axis=0, concat_axis=0, tiled=True)  218 us
    all_to_all x1, blocking collectives, summed_on_arrival(): blocks = lax.all_to_all(in_blocks(shard, dim, size), axis, 0, 0, tiled=True)  119 us
    all_to_all x1, waiting for transfers between devices, summed_on_arrival(): blocks = lax.all_to_all(in_blocks(shard, dim, size), axis, 0, 0, tiled=True)  84.8 us
    transpose x6, local copies, waits for them, and re-layouts, restore_rows(): return jnp.transpose(shaped, (0, 2, 1, 3, 4)).reshape(row_total, col_total)  16.6 us
    all_to_all x1, blocking collectives, relayout(): lax.all_to_all(lax.all_to_all(matrices[5], 'tp', split_axis=0, concat_axi...  16.3 us
    reshape x6, local copies, waits for them, and re-layouts, restore_rows(): return jnp.transpose(shaped, (0, 2, 1, 3, 4)).reshape(row_total, col_total)  15.1 us
  transfers between devices with their start and end apart: 15, of which 15 were waited for; matrix products, arithmetic and copies ran while one was open for 6% of the time, Pallas kernels for 0%

commit v1 on v0

v1 whole, which is shorter than its diff:
```python
import jax
import jax.numpy as jnp
from jax import lax
from jax.sharding import Mesh
from jax.sharding import PartitionSpec as P

D = 2048
FF = 5632
NORM_EPS = 1e-06
GR, ZL, Y, X, CORE = 2, 8, 4, 4, 2
AXES = ("gr", "zl", "y", "x", "core")
F32, BF16 = jnp.float32, jnp.bfloat16
BLOCK = FF // (ZL * Y)
ROWS = D // (GR * ZL * Y)
PAD = 72


def swap(blocks, axis):
    return lax.all_to_all(blocks, axis, split_axis=0, concat_axis=0, tiled=True)


def share(block, axis, size):
    return swap(jnp.broadcast_to(block[None], (size, *block.shape)), axis)


def relayout(gain, gate, up, down):
    rounded = jnp.stack(
        [(gain[:, None] * gate).astype(BF16), (gain[:, None] * up).astype(BF16), down.astype(BF16)]
    )
    to_y = rounded.reshape(3, ROWS, Y, BLOCK).transpose(2, 1, 0, 3).reshape(Y, ROWS, 3 * BLOCK)
    from_y = swap(to_y, "y").reshape(Y * ROWS, 3 * BLOCK)
    turned = from_y.T.reshape(X * CORE, 3 * BLOCK // 8, Y * ROWS)
    turned = jnp.pad(turned, ((0, 0), (0, PAD - 3 * BLOCK // 8), (0, 0)))
    spread = swap(swap(turned, ("x", "core")), "zl")
    both = share(spread, "gr", GR)
    wide = share(both, "x", X)
    full = share(wide, "core", CORE)
    full = full.reshape(CORE, X, GR * ZL, PAD, Y * ROWS)[:, :, :, : 3 * BLOCK // 8]
    full = full.transpose(1, 0, 3, 2, 4).reshape(3, BLOCK, D)
    return full[0], full[1], full[2]


def gathered(tokens):
    by_z = share(tokens, "zl", ZL)
    by_y = share(by_z, "y", Y)
    return by_y.transpose(1, 0, 2, 3).reshape(D, tokens.shape[1])


def summed(partial):
    width = partial.shape[1]
    to_y = partial.astype(BF16).reshape(ZL, Y, D // (ZL * Y), width).transpose(1, 0, 2, 3)
    by_y = jnp.sum(swap(to_y, "y").astype(F32), axis=0).astype(BF16)
    return jnp.sum(swap(by_y, "zl").astype(F32), axis=0)


def half_step(tokens, w_gate, w_up, w_down):
    full = gathered(tokens)
    widened = full.astype(F32)
    row_scale = (lax.rsqrt(jnp.mean(widened * widened, axis=0) + NORM_EPS) * D ** (-0.5))[None, :]
    gate = jnp.dot(w_gate, full, preferred_element_type=F32) * row_scale
    up = jnp.dot(w_up, full, preferred_element_type=F32) * row_scale
    hidden = (jax.nn.silu(gate) * up).astype(BF16)
    partial = lax.dot_general(w_down, hidden, (((0,), (0,)), ((), ())), preferred_element_type=F32)
    return (tokens.astype(F32) + 0.5 * FF ** (-0.5) * summed(partial)).astype(BF16)


def local(prompt, gain_pre, gate_pre, up_pre, down_pre, gain_post, gate_post, up_post, down_post):
    first = relayout(gain_pre, gate_pre, up_pre, down_pre)
    second = relayout(gain_post, gate_post, up_post, down_post)
    middle = half_step(prompt.T, *first)
    result = half_step(middle, *second)
    return (result.T, *first, *second)


def solution(mesh):
    fine = Mesh(mesh.devices.reshape(GR, ZL, Y, X, CORE), AXES)
    tokens = P(("gr", "x", "core"), ("zl", "y"))
    gain = P(("gr", "zl", "y"))
    trained = P(("gr", "zl", "y"), ("x", "core"))
    served = P(("zl", "y"), None)
    return jax.shard_map(
        local,
        mesh=fine,
        in_specs=(tokens, gain, trained, trained, trained, gain, trained, trained, trained),
        out_specs=(tokens,) + (served,) * 6,
        check_vma=False,
    )
```

time: 713 us -> 454 us (0.64)
  waiting for transfers between devices: 380 us -> 126 us
  blocking collectives: 135 us -> 217 us
  local copies, waits for them, and re-layouts: 82.1 us -> 39.3 us
  starting transfers between devices: 80.9 us -> 52.3 us
  between operations: 14.3 us -> 1.08 us
    all_to_all x14 -> x11, waiting for transfers between devices: 377 us -> 126 us  [swap(): return lax.all_to_all(blocks, axis, split_axis=0, concat_axis=0, tiled=True)]
    all_to_all x2 -> x9, blocking collectives: 135 us -> 217 us  [swap(): return lax.all_to_all(blocks, axis, split_axis=0, concat_axis=0, tiled=True)]
    all_to_all x14 -> x11, starting transfers between devices: 80.7 us -> 52.3 us  [swap(): return lax.all_to_all(blocks, axis, split_axis=0, concat_axis=0, tiled=True)]
    reshape x12 -> x10, local copies, waits for them, and re-layouts: 27.3 us -> 12.8 us  [the longest x2 9.04 us: relayout(): full = full.transpose(1, 0, 3, 2, 4).reshape(3, BLOCK, D)]
    transpose x6 -> x4, local copies, waits for them, and re-layouts: 16.6 us -> 7.41 us  [relayout(): full = full.transpose(1, 0, 3, 2, 4).reshape(3, BLOCK, D)]
    split x1 -> x0, local copies, waits for them, and re-layouts: 8.78 us -> none  [in_one_piece(): jnp.split(lax.all_gather(both, axis, axis=dim, tiled=True), ends, axis=al...]
    all_to_all x30 -> x6, local copies, waits for them, and re-layouts: 8.31 us -> 0.59 us  [swap(): return lax.all_to_all(blocks, axis, split_axis=0, concat_axis=0, tiled=True)]
    unnamed x16 -> x22, local copies, waits for them, and re-layouts: 10.3 us -> 2.7 us
  transfers between devices with their start and end apart: 15 -> 11, of which waited for: 15 -> 11; matrix products, arithmetic and copies ran while one was open for 6% -> 7% of each run, Pallas kernels for 0% -> 0%
where the time goes in v1:
time: 454 us; the launch traced here: 452 us
  blocking collectives  217 us (48%)
  waiting for transfers between devices  126 us (28%)
  starting transfers between devices  52.3 us (12%)
  local copies, waits for them, and re-layouts  39.3 us (9%)
  matrix products  9.12 us (2%)
  other arithmetic  6.69 us (1%)
    all_to_all x9, blocking collectives, swap(): return lax.all_to_all(blocks, axis, split_axis=0, concat_axis=0, tiled=True)  217 us
    all_to_all x11, waiting for transfers between devices, swap(): return lax.all_to_all(blocks, axis, split_axis=0, concat_axis=0, tiled=True)  126 us
    all_to_all x11, starting transfers between devices, swap(): return lax.all_to_all(blocks, axis, split_axis=0, concat_axis=0, tiled=True)  52.3 us
  transfers between devices with their start and end apart: 11, of which 11 were waited for; matrix products, arithmetic and copies ran while one was open for 7% of the time, Pallas kernels for 0%

profile of v1, /device:TPU:6, one launch (start us, length us, event | category | flops | bytes accessed | tf_op | source)
XLA Modules:
  0.0 451.9 jit_solution(5477422780115700386)
XLA Ops:
  4.7 4.5 all-to-all-start
  11.3 4.0 all-to-all-done
  15.3 3.3 all-to-all-start.10
  19.5 5.2 %all-to-all-done.10 = bf16[4,32,528]{2,1,0:T(8,128)(2,1)S(1)} async-done(((bf16[4,32,528]{2,1,0:T(8,128)(2,1)}), bf16[4,32,528]{2,1,0:T(8,128)(2,1)S(1)}, u32[]{:S(2)}, u32[]{:S(2)}) %all-to-all-start.10) | async-done | bytes 135200 | tf_op jit(solution)/shard_map/all_to_all | solution.py:19
  24.8 8.0 %all-to-all-start.1 = ((bf16[8,72,128]{2,1,0:T(8,128)(2,1)}), bf16[8,72,128]{2,1,0:T(8,128)(2,1)S(1)}, u32[]{:S(2)}, u32[]{:S(2)}) async-start(bf16[8,72,128]{2,1,0:T(8,128)(2,1)} %pad.7), calls=%async_computation.1 | async-start | bytes 294912 | tf_op jit(solution)/shard_map/all_to_all | solution.py:19
  33.0 4.0 all-to-all-done.1
  37.0 9.3 %all_to_all.100 = bf16[8,72,128]{2,1,0:T(8,128)(2,1)} all-to-all(bf16[8,72,128]{2,1,0:T(8,128)(2,1)S(1)} %pad.8), channel_id=1, replica_groups=mesh['gr'=2,'zl'=8,'y'=4,'x'=4,'core'=2] {'x','core'}, dimensions={0} | all-to-all | bytes 294912 | tf_op jit(solution)/shard_map/all_to_all | solution.py:19
  46.3 21.3 %all_to_all.101 = bf16[8,72,128]{2,1,0:T(8,128)(2,1)S(1)} all-to-all(bf16[8,72,128]{2,1,0:T(8,128)(2,1)S(1)} %all-to-all-done.1), channel_id=1, replica_groups=mesh['gr'=2,'zl'=8,'y'=4,'x'=4,'core'=2] {'zl'}, dimensions={0} | all-to-all | bytes 294912 | tf_op jit(solution)/shard_map/all_to_all | solution.py:19
  67.6 4.5 all-to-all-start.12
  72.1 12.1 %all-to-all-done.12 = bf16[8,72,128]{2,1,0:T(8,128)(2,1)S(1)} async-done(((bf16[8,72,128]{2,1,0:T(8,128)(2,1)}), bf16[8,72,128]{2,1,0:T(8,128)(2,1)S(1)}, u32[]{:S(2)}, u32[]{:S(2)}) %all-to-all-start.12) | async-done | bytes 147488 | tf_op jit(solution)/shard_map/all_to_all | solution.py:19
  84.2 25.4 %all_to_all.102 = bf16[2,8,72,128]{3,1,2,0:T(8,128)(2,1)S(1)} all-to-all(bf16[2,8,72,128]{3,1,2,0:T(8,128)(2,1)S(1)} %broadcast_in_dim.20), channel_id=1, replica_groups=mesh['gr'=2,'zl'=8,'y'=4,'x'=4,'core'=2] {'gr'}, dimensions={0} | all-to-all | bytes 589824 | tf_op jit(solution)/shard_map/all_to_all | solution.py:19
  110.5 8.0 %all-to-all-start.6 = ((bf16[8,64,512]{2,1,0:T(8,128)(2,1)}), bf16[8,64,512]{2,1,0:T(8,128)(2,1)S(1)}, u32[]{:S(2)}, u32[]{:S(2)}) async-start(bf16[8,64,512]{2,1,0:T(8,128)(2,1)} %broadcast_in_dim.23), calls=%async_computation.6 | async-start | bytes 1048576 | tf_op jit(solution)/shard_map/all_to_all | solution.py:19
  118.5 28.9 %all-to-all-done.6 = bf16[8,64,512]{2,1,0:T(8,128)(2,1)S(1)} async-done(((bf16[8,64,512]{2,1,0:T(8,128)(2,1)}), bf16[8,64,512]{2,1,0:T(8,128)(2,1)S(1)}, u32[]{:S(2)}, u32[]{:S(2)}) %all-to-all-start.6) | async-done | bytes 524320 | tf_op jit(solution)/shard_map/all_to_all | solution.py:19
  147.5 14.0 %all_to_all.103 = bf16[4,2,8,72,128]{4,2,1,3,0:T(8,128)(2,1)S(1)} all-to-all(bf16[4,2,8,72,128]{4,2,1,3,0:T(8,128)(2,1)S(1)} %broadcast_in_dim.21), channel_id=1, replica_groups=mesh['gr'=2,'zl'=8,'y'=4,'x'=4,'core'=2] {'x'}, dimensions={0} | all-to-all | bytes 2359296 | tf_op jit(solution)/shard_map/all_to_all | solution.py:19
  161.9 6.6 %all_to_all.104 = bf16[2,4,2,8,72,128]{5,3,2,4,1,0:T(8,128)(2,1)} all-to-all(bf16[2,4,2,8,72,128]{5,3,2,4,1,0:T(8,128)(2,1)S(1)} %broadcast_in_dim.22), channel_id=1, replica_groups=mesh['gr'=2,'zl'=8,'y'=4,'x'=4,'core'=2] {'core'}, dimensions={0} | all-to-all | bytes 4718592 | tf_op jit(solution)/shard_map/all_to_all | solution.py:19
  168.4 1.6 broadcast_in_dim.24
  170.0 3.6 all-to-all-start.7
  173.7 2.0 slice_bitcast_fusion.1
  175.7 1.7 copy.50
  177.4 4.5 %reshape.98 = bf16[3,176,2048]{2,1,0:T(8,128)(2,1)} reshape(bf16[4,2,66,16,128]{4,3,2,1,0:T(8,128)(2,1)} %copy.50) | data formatting | bytes 4325376 | tf_op jit(solution)/shard_map/reshape | solution.py:39
  181.9 2.9 slice_bitcast_fusion.6
  184.8 15.8 %all-to-all-done.7 = bf16[4,8,64,512]{3,2,1,0:T(8,128)(2,1)S(1)} async-done(((bf16[4,8,64,512]{3,2,1,0:T(8,128)(2,1)}), bf16[4,8,64,512]{3,2,1,0:T(8,128)(2,1)S(1)}, u32[]{:S(2)}, u32[]{:S(2)}) %all-to-all-start.7) | async-done | bytes 2097184 | tf_op jit(solution)/shard_map/all_to_all | solution.py:19
  201.2 3.4 all-to-all-start.13
  205.5 1.3 copy-done.1
  206.9 1.3 convolution_multiply_fusion.3
  208.1 3.3 convolution_convert_fusion.1
  211.4 1.5 copy.67
  212.9 6.0 %all-to-all-done.13 = bf16[2,8,72,128]{3,1,2,0:T(8,128)(2,1)S(1)} async-done(((bf16[2,8,72,128]{3,1,2,0:T(8,128)(2,1)}), bf16[2,8,72,128]{3,1,2,0:T(8,128)(2,1)S(1)}, u32[]{:S(2)}, u32[]{:S(2)}) %all-to-all-start.13) | async-done | bytes 294944 | tf_op jit(solution)/shard_map/all_to_all | solution.py:19
  218.9 3.6 all-to-all-start.8
  222.6 24.9 %all-to-all-done.8 = bf16[4,8,64,512]{3,2,1,0:T(8,128)(2,1)S(1)} async-done(((bf16[4,8,64,512]{3,2,1,0:T(8,128)(2,1)}), bf16[4,8,64,512]{3,2,1,0:T(8,128)(2,1)S(1)}, u32[]{:S(2)}, u32[]{:S(2)}) %all-to-all-start.8) | async-done | bytes 2097184 | tf_op jit(solution)/shard_map/all_to_all | solution.py:19
  248.7 5.6 %all-to-all-start.14 = ((bf16[4,2,8,72,128]{4,2,1,3,0:T(8,128)(2,1)}), bf16[4,2,8,72,128]{4,2,1,3,0:T(8,128)(2,1)S(1)}, u32[]{:S(2)}, u32[]{:S(2)}) async-start(bf16[4,2,8,72,128]{4,2,1,3,0:T(8,128)(2,1)} %broadcast_in_dim.26), calls=%async_computation.14 | async-start | bytes 2359296 | tf_op jit(solution)/shard_map/all_to_all | solution.py:19
  255.5 11.0 %all-to-all-done.14 = bf16[4,2,8,72,128]{4,2,1,3,0:T(8,128)(2,1)S(1)} async-done(((bf16[4,2,8,72,128]{4,2,1,3,0:T(8,128)(2,1)}), bf16[4,2,8,72,128]{4,2,1,3,0:T(8,128)(2,1)S(1)}, u32[]{:S(2)}, u32[]{:S(2)}) %all-to-all-start.14) | async-done | bytes 1179680 | tf_op jit(solution)/shard_map/all_to_all | solution.py:19
  266.5 45.6 %all_to_all.105 = bf16[8,64,512]{2,1,0:T(8,128)(2,1)} all-to-all(bf16[8,64,512]{2,1,0:T(8,128)(2,1)} %reduce_sum.61), channel_id=1, replica_groups=mesh['gr'=2,'zl'=8,'y'=4,'x'=4,'core'=2] {'zl'}, dimensions={0} | all-to-all | bytes 1048576 | tf_op jit(solution)/shard_map/all_to_all | solution.py:19
  312.1 1.7 broadcast_in_dim.27
  313.8 3.9 all-to-all-start.15
  317.9 2.9 all-to-all-done.15
  320.8 33.1 %all_to_all.106 = bf16[8,64,512]{2,1,0:T(8,128)(2,1)S(1)} all-to-all(bf16[8,64,512]{2,1,0:T(8,128)(2,1)S(1)} %broadcast_in_dim.28), channel_id=1, replica_groups=mesh['gr'=2,'zl'=8,'y'=4,'x'=4,'core'=2] {'zl'}, dimensions={0} | all-to-all | bytes 1048576 | tf_op jit(solution)/shard_map/all_to_all | solution.py:19
  353.9 1.6 broadcast_in_dim.29
  355.5 3.8 all-to-all-start.17
  359.3 2.0 slice_bitcast_fusion
  361.3 1.7 copy.59
  363.0 4.5 %reshape.105 = bf16[3,176,2048]{2,1,0:T(8,128)(2,1)} reshape(bf16[4,2,66,16,128]{4,3,2,1,0:T(8,128)(2,1)} %copy.59) | data formatting | bytes 4325376 | tf_op jit(solution)/shard_map/reshape | solution.py:39
  367.5 2.9 slice_bitcast_fusion.3
  370.4 11.6 %all-to-all-done.17 = bf16[4,8,64,512]{3,2,1,0:T(8,128)(2,1)S(1)} async-done(((bf16[4,8,64,512]{3,2,1,0:T(8,128)(2,1)}), bf16[4,8,64,512]{3,2,1,0:T(8,128)(2,1)S(1)}, u32[]{:S(2)}, u32[]{:S(2)}) %all-to-all-start.17) | async-done | bytes 2097184 | tf_op jit(solution)/shard_map/all_to_all | solution.py:19
  382.8 1.3 copy-done.2
  385.4 3.3 convolution_convert_fusion
  388.9 24.5 %all_to_all.107 = bf16[4,8,64,512]{3,2,1,0:T(8,128)(2,1)S(1)} all-to-all(bf16[4,8,64,512]{3,2,1,0:T(8,128)(2,1)S(1)} %bitcast.75), channel_id=1, replica_groups=mesh['gr'=2,'zl'=8,'y'=4,'x'=4,'core'=2] {'y'}, dimensions={0} | all-to-all | bytes 4194304 | tf_op jit(solution)/shard_map/all_to_all | solution.py:19
  413.8 37.5 %all_to_all.108 = bf16[8,64,512]{2,1,0:T(8,128)(2,1)S(1)} all-to-all(bf16[8,64,512]{2,1,0:T(8,128)(2,1)S(1)} %reduce_sum.64), channel_id=1, replica_groups=mesh['gr'=2,'zl'=8,'y'=4,'x'=4,'core'=2] {'zl'}, dimensions={0} | all-to-all | bytes 1048576 | tf_op jit(solution)/shard_map/all_to_all | solution.py:19
  (71 shorter events, 16.0 us)
Async XLA Ops:
  0.6 8.5 %copy-start.7 = (f32[32,704]{1,0:T(8,128)S(1)}, f32[32,704]{1,0:T(8,128)}, u32[]{:S(2)}) copy-start(f32[32,704]{1,0:T(8,128)} %param.17) | copy-start | bytes 270340
  0.6 8.7 %copy-start.9 = (f32[32,704]{1,0:T(8,128)S(1)}, f32[32,704]{1,0:T(8,128)}, u32[]{:S(2)}) copy-start(f32[32,704]{1,0:T(8,128)} %param.16) | copy-start | bytes 270340
  0.7 8.7 %copy-start.8 = (f32[32,704]{1,0:T(8,128)S(1)}, f32[32,704]{1,0:T(8,128)}, u32[]{:S(2)}) copy-start(f32[32,704]{1,0:T(8,128)} %param.15) | copy-start | bytes 270340
  0.7 8.7 %copy-start.10 = (f32[32]{0:T(128)S(1)}, f32[32]{0:T(128)}, u32[]{:S(2)}) copy-start(f32[32]{0:T(128)} %param.14) | copy-start | bytes 388
  4.7 10.6 %all-to-all-start = ((bf16[4,32,528]{2,1,0:T(8,128)(2,1)}), bf16[4,32,528]{2,1,0:T(8,128)(2,1)S(1)}, u32[]{:S(2)}, u32[]{:S(2)}) async-start(bf16[4,32,528]{2,1,0:T(8,128)(2,1)} %reshape.94), calls=%async_computation | async-start | bytes 327680 | tf_op jit(solution)/shard_map/all_to_all | solution.py:19
  15.3 9.5 %all-to-all-start.10 = ((bf16[4,32,528]{2,1,0:T(8,128)(2,1)}), bf16[4,32,528]{2,1,0:T(8,128)(2,1)S(1)}, u32[]{:S(2)}, u32[]{:S(2)}) async-start(bf16[4,32,528]{2,1,0:T(8,128)(2,1)} %reshape.101), calls=%async_computation.10 | async-start | bytes 327680 | tf_op jit(solution)/shard_map/all_to_all | solution.py:19
  18.7 91.0 %copy-start.6 = (bf16[512,64]{0,1:T(8,128)(2,1)S(1)}, bf16[512,64]{0,1:T(8,128)(2,1)}, u32[]{:S(2)}) copy-start(bf16[512,64]{0,1:T(8,128)(2,1)} %param.9) | copy-start | bytes 196612
  24.8 12.2 %all-to-all-start.1 = ((bf16[8,72,128]{2,1,0:T(8,128)(2,1)}), bf16[8,72,128]{2,1,0:T(8,128)(2,1)S(1)}, u32[]{:S(2)}, u32[]{:S(2)}) async-start(bf16[8,72,128]{2,1,0:T(8,128)(2,1)} %pad.7), calls=%async_computation.1 | async-start | bytes 294912 | tf_op jit(solution)/shard_map/all_to_all | solution.py:19
  67.6 16.6 %all-to-all-start.12 = ((bf16[8,72,128]{2,1,0:T(8,128)(2,1)}), bf16[8,72,128]{2,1,0:T(8,128)(2,1)S(1)}, u32[]{:S(2)}, u32[]{:S(2)}) async-start(bf16[8,72,128]{2,1,0:T(8,128)(2,1)} %all_to_all.100), calls=%async_computation.12 | async-start | bytes 294912 | tf_op jit(solution)/shard_map/all_to_all | solution.py:19
  110.5 36.9 %all-to-all-start.6 = ((bf16[8,64,512]{2,1,0:T(8,128)(2,1)}), bf16[8,64,512]{2,1,0:T(8,128)(2,1)S(1)}, u32[]{:S(2)}, u32[]{:S(2)}) async-start(bf16[8,64,512]{2,1,0:T(8,128)(2,1)} %broadcast_in_dim.23), calls=%async_computation.6 | async-start | bytes 1048576 | tf_op jit(solution)/shard_map/all_to_all | solution.py:19
  170.0 30.5 %all-to-all-start.7 = ((bf16[4,8,64,512]{3,2,1,0:T(8,128)(2,1)}), bf16[4,8,64,512]{3,2,1,0:T(8,128)(2,1)S(1)}, u32[]{:S(2)}, u32[]{:S(2)}) async-start(bf16[4,8,64,512]{3,2,1,0:T(8,128)(2,1)} %broadcast_in_dim.24), calls=%async_computation.7 | async-start | bytes 4194304 | tf_op jit(solution)/shard_map/all_to_all | solution.py:19
  184.8 20.8 %copy-start.3 = (bf16[176,2048]{1,0:T(8,128)(2,1)}, bf16[176,2048]{1,0:T(8,128)(2,1)S(1)}, u32[]{:S(2)}) copy-start(bf16[176,2048]{1,0:T(8,128)(2,1)S(1)} %get-tuple-element.10) | copy-start | bytes 2162692
  201.2 17.6 %all-to-all-start.13 = ((bf16[2,8,72,128]{3,1,2,0:T(8,128)(2,1)}), bf16[2,8,72,128]{3,1,2,0:T(8,128)(2,1)S(1)}, u32[]{:S(2)}, u32[]{:S(2)}) async-start(bf16[2,8,72,128]{3,1,2,0:T(8,128)(2,1)} %broadcast_in_dim.25), calls=%async_computation.13 | async-start | bytes 589824 | tf_op jit(solution)/shard_map/all_to_all | solution.py:19
  205.5 1.3 copy-start.1
  218.9 28.6 %all-to-all-start.8 = ((bf16[4,8,64,512]{3,2,1,0:T(8,128)(2,1)}), bf16[4,8,64,512]{3,2,1,0:T(8,128)(2,1)S(1)}, u32[]{:S(2)}, u32[]{:S(2)}) async-start(bf16[4,8,64,512]{3,2,1,0:T(8,128)(2,1)} %bitcast.70), calls=%async_computation.8 | async-start | bytes 4194304 | tf_op jit(solution)/shard_map/all_to_all | solution.py:19
  248.7 17.8 %all-to-all-start.14 = ((bf16[4,2,8,72,128]{4,2,1,3,0:T(8,128)(2,1)}), bf16[4,2,8,72,128]{4,2,1,3,0:T(8,128)(2,1)S(1)}, u32[]{:S(2)}, u32[]{:S(2)}) async-start(bf16[4,2,8,72,128]{4,2,1,3,0:T(8,128)(2,1)} %broadcast_in_dim.26), calls=%async_computation.14 | async-start | bytes 2359296 | tf_op jit(solution)/shard_map/all_to_all | solution.py:19
  313.8 4.0 copy-start.5
  313.8 7.0 %all-to-all-start.15 = ((bf16[2,4,2,8,72,128]{5,3,2,4,1,0:T(8,128)(2,1)}), bf16[2,4,2,8,72,128]{5,3,2,4,1,0:T(8,128)(2,1)S(1)}, u32[]{:S(2)}, u32[]{:S(2)}) async-start(bf16[2,4,2,8,72,128]{5,3,2,4,1,0:T(8,128)(2,1)} %broadcast_in_dim.27), calls=%async_computation.15 | async-start | bytes 4718592 | tf_op jit(solution)/shard_map/all_to_all | solution.py:19
  320.8 34.7 %copy-start = (bf16[2,4,2,8,72,128]{5,3,2,4,1,0:T(8,128)(2,1)}, bf16[2,4,2,8,72,128]{5,3,2,4,1,0:T(8,128)(2,1)S(1)}, u32[]{:S(2)}) copy-start(bf16[2,4,2,8,72,128]{5,3,2,4,1,0:T(8,128)(2,1)S(1)} %all-to-all-done.15) | copy-start | bytes 7077892
  355.5 26.4 %all-to-all-start.17 = ((bf16[4,8,64,512]{3,2,1,0:T(8,128)(2,1)}), bf16[4,8,64,512]{3,2,1,0:T(8,128)(2,1)S(1)}, u32[]{:S(2)}, u32[]{:S(2)}) async-start(bf16[4,8,64,512]{3,2,1,0:T(8,128)(2,1)} %broadcast_in_dim.29), calls=%async_computation.17 | async-start | bytes 4194304 | tf_op jit(solution)/shard_map/all_to_all | solution.py:19
  370.4 12.4 %copy-start.4 = (bf16[176,2048]{1,0:T(8,128)(2,1)}, bf16[176,2048]{1,0:T(8,128)(2,1)S(1)}, u32[]{:S(2)}) copy-start(bf16[176,2048]{1,0:T(8,128)(2,1)S(1)} %get-tuple-element.7) | copy-start | bytes 2162692
  382.8 1.3 copy-start.2
